TPU v7x, 32 devices: a whole 2x2x4 slice. The times are simulated.
32 devices in a mesh: sp: 8 (over z, x), tp: 4 (over y, core).
Axes of the slice: x: 2, y: 2, z: 4, core: 2. Of those that a mesh axis runs over, the one named last changes fastest.
Arguments:
- residual_in: bfloat16 [4096, 2048], P('sp'), may hold values from -6 to 6
- gate_in: bfloat16 [4096, 2048], P('sp', 'tp'), may hold values from -6 to 6
- value_in: bfloat16 [4096, 2048], P('sp', 'tp'), may hold values from -6 to 6
- conv_weight: float32 [4, 2048], P(None, 'tp'), may hold values from -3 to 3
- rate_weight: bfloat16 [32, 64, 64], P('tp'), may hold values from -0.75 to 0.75
- input_weight: bfloat16 [32, 64, 64], P('tp'), may hold values from -0.75 to 0.75
- decay_base: float32 [2048], P('tp'), may hold values from 3.0517578e-06 to 0.015, as said below
- step_scale: float32 [4096, 2048], P('sp', 'tp'), may hold values from 0.25 to 57344, as said below
- out_weight: bfloat16 [2048, 2048], P('tp'), may hold values from -0.375 to 0.375
- norm_gain: float32 [2048], replicated, may hold values from 0.1 to 1.9
- up_weight: bfloat16 [2048, 8192], P('sp', 'tp'), may hold values from -0.125 to 0.125
- down_weight: bfloat16 [2048, 8192], P('sp', 'tp'), may hold values from -0.0625 to 0.0625
Outputs:
- block_out: bfloat16 [4096, 2048], P(('sp', 'tp'))
Inputs may be any that keep to these rules, and one draw needn't show every extreme that they name: `decay_base`: positive. `step_scale`: positive.
All inputs are finite; a program needn't handle non-finite values.
Results may differ from a plain program's by a relative error of at most 0.018.
Values may be sent and summed in bfloat16 or wider, within the bound.
A program may use at most 128 MiB of HBM per device.

v0:
```python
import math

import jax
import jax.numpy as jnp
from jax import lax
from jax.sharding import PartitionSpec as P


def shifted(block, axis, distance):
    devices = range(lax.axis_size(axis))
    route = [(i - distance, i) for i in devices if i - distance in devices]
    return lax.ppermute(block, axis, route)


def carried_in(part, axis, combine, identity):
    place = lax.axis_index(axis)
    gathered = jax.tree.map(lambda a: lax.all_gather(a, axis), part)
    state = jax.tree.map(lambda a, e: jnp.zeros_like(a) + jnp.asarray(e, a.dtype), part, identity)

    def one(turn, state):
        return combine(
            state, jax.tree.map(lambda a: lax.dynamic_index_in_dim(a, turn, 0, False), gathered)
        )

    return lax.fori_loop(0, place, one, state)


def chain_join(earlier, later):
    return (earlier[0] * later[0], later[0] * earlier[1] + later[1])


def rounded(term):
    return lax.optimization_barrier(term.astype(jnp.bfloat16)).astype(jnp.float32)


def settle_rows(rows_in, norm_gain):
    widened = rows_in.astype(jnp.float32)
    factor = lax.rsqrt(jnp.mean(widened * widened, axis=-1, keepdims=True) + 1e-06)
    return (widened * factor * norm_gain).astype(jnp.bfloat16)


def step_rows(carry, inputs):
    keep_row, drive_row = inputs
    new_product = carry[0] * keep_row
    new_state = keep_row * carry[1] + drive_row
    return ((new_product, new_state), (new_product, new_state))


def local(
    residual_in,
    gate_in,
    value_in,
    conv_weight,
    rate_weight,
    input_weight,
    decay_base,
    step_scale,
    out_weight,
    norm_gain,
    up_weight,
    down_weight,
):
    row_count = value_in.shape[0]
    tap_count = conv_weight.shape[0]
    channel_count = value_in.shape[1]
    earlier_rows = shifted(value_in[row_count - tap_count + 1 :], "sp", 1)
    padded = jnp.concatenate([earlier_rows, value_in], axis=0).astype(jnp.float32)
    filtered_rows = jnp.zeros(value_in.shape, jnp.float32)
    for offset in range(tap_count):
        filtered_rows = filtered_rows + padded[offset : offset + row_count] * conv_weight[offset]
    smoothed = filtered_rows.astype(jnp.bfloat16)
    grouped = smoothed.reshape(row_count, rate_weight.shape[0], rate_weight.shape[1])
    rate_gate = jax.nn.sigmoid(
        jnp.einsum("tnd,nde->tne", grouped, rate_weight, preferred_element_type=jnp.float32)
    ).reshape(row_count, -1)
    input_gate = jax.nn.sigmoid(
        jnp.einsum("tnd,nde->tne", grouped, input_weight, preferred_element_type=jnp.float32)
    ).reshape(row_count, -1)
    log_keep = -8.0 * step_scale * rate_gate * decay_base[None, :]
    drive = jnp.sqrt(-jnp.expm1(2.0 * log_keep)) * input_gate * smoothed.astype(jnp.float32)
    block_rows = math.gcd(row_count, 16)
    block_count = row_count // block_rows
    keep_blocks = (
        jnp.exp(log_keep).reshape(block_count, block_rows, channel_count).transpose(1, 0, 2)
    )
    drive_blocks = drive.reshape(block_count, block_rows, channel_count).transpose(1, 0, 2)
    start_carry = (
        jnp.ones((block_count, channel_count), jnp.float32),
        jnp.zeros((block_count, channel_count), jnp.float32),
    )
    final_carry, inner = lax.scan(step_rows, start_carry, (keep_blocks, drive_blocks))
    inner_products, inner_states = inner
    prefix_products, prefix_states = lax.associative_scan(chain_join, final_carry, axis=0)
    carried = carried_in(
        (prefix_products[-1], prefix_states[-1]),
        "sp",
        chain_join,
        (jnp.ones_like(prefix_products[-1]), jnp.zeros_like(prefix_states[-1])),
    )
    entry_products = jnp.concatenate(
        [jnp.ones((1, channel_count), jnp.float32), prefix_products[:-1]], axis=0
    )
    entry_states = jnp.concatenate(
        [jnp.zeros((1, channel_count), jnp.float32), prefix_states[:-1]], axis=0
    )
    entering = entry_states + entry_products * carried[1][None, :]
    carry_state = (
        (inner_states + inner_products * entering[None, :, :])
        .transpose(1, 0, 2)
        .reshape(row_count, channel_count)
    )
    gated = (jax.nn.gelu(gate_in.astype(jnp.float32), approximate=True) * carry_state).astype(
        jnp.bfloat16
    )
    group_rows = row_count // lax.axis_size("tp")
    own_start = lax.axis_index("tp") * group_rows
    mixed = lax.psum(
        rounded(jnp.dot(gated, out_weight, preferred_element_type=jnp.float32)).astype(
            jnp.bfloat16
        ),
        "tp",
    ).astype(jnp.float32)
    updated = (residual_in.astype(jnp.float32) + mixed).astype(jnp.bfloat16)
    normed = settle_rows(updated, norm_gain)
    own_updated = lax.dynamic_slice_in_dim(updated, own_start, group_rows, 0)
    lifted = jnp.dot(
        normed,
        lax.all_gather(up_weight, "sp", axis=0, tiled=True),
        preferred_element_type=jnp.float32,
    )
    activated = jnp.square(jax.nn.relu(lifted)).astype(jnp.bfloat16)
    partial_rows = lax.dot_general(
        activated,
        lax.all_gather(down_weight, "sp", axis=0, tiled=True),
        (((1,), (1,)), ((), ())),
        preferred_element_type=jnp.float32,
    )
    summed = lax.psum_scatter(
        rounded(partial_rows).astype(jnp.bfloat16), "tp", scatter_dimension=0, tiled=True
    ).astype(jnp.float32)
    return (own_updated.astype(jnp.float32) + summed).astype(jnp.bfloat16)


def solution(mesh):
    in_specs = (
        P("sp", None),
        P("sp", "tp"),
        P("sp", "tp"),
        P(None, "tp"),
        P("tp", None, None),
        P("tp", None, None),
        P("tp"),
        P("sp", "tp"),
        P("tp", None),
        P(),
        P("sp", "tp"),
        P("sp", "tp"),
    )
    out_specs = P(("sp", "tp"), None)
    return jax.shard_map(local, mesh=mesh, in_specs=in_specs, out_specs=out_specs, check_vma=False)
```

profile of v0, /device:TPU:0, one launch (start us, length us, event | category | flops | bytes accessed | tf_op | source)
XLA Modules:
  0.0 487.0 jit_solution(7108042623336338407)
XLA Ops:
  8.4 4.9 %collective-permute-start = (bf16[3,512]{0,1:T(8,128)(2,1)S(1)}, bf16[3,512]{0,1:T(8,128)(2,1)S(1)}, u32[]{:S(2)}, u32[]{:S(2)}) collective-permute-start(bf16[3,512]{0,1:T(8,128)(2,1)S(1)} %copy.31), channel_id=1, source_target_pairs={{0,4},{4,8},{8,12},{12,16},{16,20},{20,24},{24,28},{1,5},{5,9},{9,... | collective-permute-start | bytes 9224 | tf_op jit(solution)/shard_map/ppermute | solution.py:12
  14.2 2.0 copy.32
  16.2 1.6 copy.30
  22.1 2.7 fusion.24
  24.7 2.6 copy.34
  28.7 92.3 %while.30 = (s32[]{:T(128)}, f32[32,512]{1,0:T(8,128)S(1)}, f32[32,512]{1,0:T(8,128)S(1)}, f32[16,32,512]{2,0,1:T(8,128)}, f32[16,32,512]{2,0,1:T(8,128)}, /*ind...) while((s32[]{:T(128)}, f32[32,512]{1,0:T(8,128)S(1)}, ...), condition=%wide.region_1.2_spmd.clone, body=%wide.region_0.1_spmd.clone.sunk | while | flops 81923 | bytes 1179763 | solution.py:91
  30.1 2.1 dynamic_update_slice.12
  32.3 2.1 dynamic_update_slice.11
  35.9 2.1 dynamic_update_slice.12
  38.1 2.1 dynamic_update_slice.11
  41.7 2.1 dynamic_update_slice.12
  43.9 2.1 dynamic_update_slice.11
  47.5 2.1 dynamic_update_slice.12
  49.7 2.1 dynamic_update_slice.11
  53.3 2.1 dynamic_update_slice.12
  55.5 2.1 dynamic_update_slice.11
  59.1 2.1 dynamic_update_slice.12
  61.3 2.1 dynamic_update_slice.11
  64.8 2.1 dynamic_update_slice.12
  67.1 2.1 dynamic_update_slice.11
  70.6 2.1 dynamic_update_slice.12
  72.8 2.1 dynamic_update_slice.11
  76.4 2.1 dynamic_update_slice.12
  78.6 2.1 dynamic_update_slice.11
  82.2 2.1 dynamic_update_slice.12
  84.4 2.1 dynamic_update_slice.11
  87.9 2.1 dynamic_update_slice.12
  90.1 2.1 dynamic_update_slice.11
  93.7 2.1 dynamic_update_slice.12
  95.9 2.1 dynamic_update_slice.11
  99.4 2.1 dynamic_update_slice.12
  101.6 2.1 dynamic_update_slice.11
  105.2 2.1 dynamic_update_slice.12
  107.4 2.1 dynamic_update_slice.11
  110.9 2.1 dynamic_update_slice.12
  113.1 2.1 dynamic_update_slice.11
  116.7 2.1 dynamic_update_slice.12
  118.9 2.1 dynamic_update_slice.11
  125.3 26.6 %all-gather.1 = f32[8,1,512]{2,1,0:T(1,128)S(1)} all-gather(f32[1,1,512]{2,1,0:T(1,128)S(1)} %get-tuple-element.192), channel_id=1, replica_groups=mesh['sp'=8,'tp'=4] {'sp'}, dimensions={0}, use_global_device_ids=true | all-gather | bytes 18432 | tf_op jit(solution)/shard_map/all_gather | solution.py:17
  151.9 26.1 %all-gather = f32[8,1,512]{2,1,0:T(1,128)S(1)} all-gather(f32[1,1,512]{2,1,0:T(1,128)S(1)} %get-tuple-element.193), channel_id=1, replica_groups=mesh['sp'=8,'tp'=4] {'sp'}, dimensions={0}, use_global_device_ids=true | all-gather | bytes 18432 | tf_op jit(solution)/shard_map/all_gather | solution.py:17
  180.2 2.6 convolution_convert_fusion.1
  184.2 47.5 %all-reduce.24.cloned.1.call-done = bf16[512,2048]{1,0:T(8,128)(2,1)} async-done(((bf16[512,2048]{1,0:T(8,128)(2,1)}), bf16[512,2048]{1,0:T(8,128)(2,1)}) %all-reduce.24.cloned.1.call-update) | async-done | bytes 2097168 | tf_op jit(solution)/shard_map/psum | solution.py:117
  231.8 4.6 fusion.1
  236.3 70.7 %all-gather.5.cloned.1.call-done = bf16[2048,2048]{1,0:T(8,128)(2,1)} async-done(((bf16[256,2048]{1,0:T(8,128)(2,1)}), bf16[2048,2048]{1,0:T(8,128)(2,1)}) %all-gather.5.cloned.1.call-update) | async-done | bytes 8388624 | tf_op jit(solution)/shard_map/all_gather | solution.py:128
  307.0 124.4 %all-gather.7.cloned.1.call-done = bf16[2048,2048]{1,0:T(8,128)(2,1)} async-done(((bf16[256,2048]{1,0:T(8,128)(2,1)}), bf16[2048,2048]{1,0:T(8,128)(2,1)}) %all-gather.7.cloned.1.call-update) | async-done | bytes 8388624 | tf_op jit(solution)/shard_map/all_gather | solution.py:134
  431.4 16.6 %convolution_convert_fusion = bf16[512,2048]{1,0:T(8,128)(2,1)} fusion(bf16[2048,2048]{1,0:T(8,128)(2,1)} %all-gather.7.cloned.1.call-done, bf16[2048,2048]{1,0:T(8,128)(2,1)} %all-gather.5.cloned.1.call-done, bf16[512,2048]{1,0:T(8,128)(2,1)} %get-tuple-element.157, f32[2048]{0:T(1024)S(1)} %copy-done.7, f32[512]{0:T(512)S(1)} %add_rsqrt_fusion), kind=kOutput, calls=%fused_computation.17 | convolution fusion | flops 8598323200 | bytes 20981760 | tf_op jit(solution)/shard_map/dot_general | solution.py:132
  448.0 29.5 %reduce-scatter.2.cloned.1.call-done = bf16[128,2048]{1,0:T(8,128)(2,1)} async-done(((bf16[512,2048]{1,0:T(8,128)(2,1)}), bf16[128,2048]{1,0:T(8,128)(2,1)}) %reduce-scatter.2.cloned.1.call-update) | async-done | bytes 524304 | tf_op jit(solution)/shard_map/reduce_scatter | solution.py:138
  477.4 2.1 add_convert_fusion.1
  (181 shorter events, 39.0 us)
Async XLA Ops:
  7.4 172.8 %copy-start = (bf16[512,2048]{1,0:T(8,128)(2,1)S(1)}, bf16[512,2048]{1,0:T(8,128)(2,1)}, u32[]{:S(2)}) copy-start(bf16[512,2048]{1,0:T(8,128)(2,1)} %param.24) | copy-start | bytes 6291460
  7.4 224.4 %all-reduce.24.cloned.1.call-start = ((), (), s32[]{:S(2)}) async-start(), calls=%async_computation.1 | async-start | bytes 4194304 | tf_op jit(solution)/shard_map/psum | solution.py:117
  8.4 9.4 %collective-permute-start = (bf16[3,512]{0,1:T(8,128)(2,1)S(1)}, bf16[3,512]{0,1:T(8,128)(2,1)S(1)}, u32[]{:S(2)}, u32[]{:S(2)}) collective-permute-start(bf16[3,512]{0,1:T(8,128)(2,1)S(1)} %copy.31), channel_id=1, source_target_pairs={{0,4},{4,8},{8,12},{12,16},{16,20},{20,24},{24,28},{1,5},{5,9},{9,... | collective-permute-start | bytes 9224 | tf_op jit(solution)/shard_map/ppermute | solution.py:12
  19.1 1.3 copy-start.5
  20.5 0.9 copy-start.6
  21.4 0.7 copy-start.4
  24.7 2.6 copy-start.1
  121.0 57.2 %copy-start.2 = (f32[16,32,512]{2,0,1:T(8,128)S(1)}, f32[16,32,512]{2,0,1:T(8,128)}, u32[]{:S(2)}) copy-start(f32[16,32,512]{2,0,1:T(8,128)} %get-tuple-element.90) | copy-start | bytes 3145732
  178.1 1.6 copy-start.3
  182.8 124.2 %all-gather.5.cloned.1.call-start = ((), (), s32[]{:S(2)}) async-start(), calls=%async_computation.2 | async-start | bytes 9437184 | tf_op jit(solution)/shard_map/all_gather | solution.py:128
  183.4 248.0 %all-gather.7.cloned.1.call-start = ((), (), s32[]{:S(2)}) async-start(), calls=%async_computation.3 | async-start | bytes 9437184 | tf_op jit(solution)/shard_map/all_gather | solution.py:134
  184.0 247.4 %copy-start.7 = (f32[2048]{0:T(1024)S(1)}, f32[2048]{0:T(1024)}, u32[]{:S(2)}) copy-start(f32[2048]{0:T(1024)} %param.25) | copy-start | bytes 24580
  184.0 293.4 %reduce-scatter.2.cloned.1.call-start = ((), (), s32[]{:S(2)}) async-start(), calls=%async_computation.4 | async-start | bytes 2621440 | tf_op jit(solution)/shard_map/reduce_scatter | solution.py:138
Sparse Core Ops, SparseCore 0:
  182.9 48.7 all-reduce.23
  448.1 29.3 reduce-scatter.1
Sparse Core Ops, SparseCore 1:
  185.4 121.5 all-gather.4
  309.0 122.3 all-gather.6
where the time goes:
time: 489 us; the launch traced here: 487 us
  waiting for transfers between devices  273 us (56%)
  local copies, waits for them, and re-layouts  104 us (21%)
  blocking collectives  52.7 us (11%)
  matrix products  20.2 us (4%)
  other arithmetic  15.8 us (3%)
  between operations  15.3 us (3%)
  starting transfers between devices  5.19 us (1%)
    all_gather x1, waiting for transfers between devices, local(): lax.all_gather(down_weight, 'sp', axis=0, tiled=True)  124 us
    all_gather x1, waiting for transfers between devices, local(): lax.all_gather(up_weight, 'sp', axis=0, tiled=True)  70.7 us
    dynamic_update_slice x64, local copies, waits for them, and re-layouts, local(): lax.scan(step_rows, start_carry, (keep_blocks, drive_blocks))  70.1 us
    all_gather x2, blocking collectives, carried_in(): gathered = jax.tree.map(lambda a: lax.all_gather(a, axis), part)  52.7 us
    psum x1, waiting for transfers between devices, local(): lax.psum(rounded(jnp.dot(gated, out_weight, preferred_element_type=jnp.fl...  47.5 us
    reduce_scatter x1, waiting for transfers between devices, local(): lax.psum_scatter(rounded(partial_rows).astype(jnp.bfloat16), 'tp', scatte...  29.5 us
    dynamic_slice x16, local copies, waits for them, and re-layouts, local(): lax.scan(step_rows, start_carry, (keep_blocks, drive_blocks))  21 us
    dot_general x1, matrix products, local(): lax.dot_general(activated, lax.all_gather(down_weight, 'sp', axis=0, tile...  16.6 us
  transfers between devices with their start and end apart: 5, of which 4 were waited for; matrix products, arithmetic and copies ran while one was open for 2% of the time, Pallas kernels for 0%

commit v1 on v0

v1 whole, which is shorter than its diff:
```python
import functools

import jax
import jax.numpy as jnp
from jax import lax
from jax.experimental import pallas as pl
from jax.experimental.pallas import tpu as pltpu
from jax.sharding import PartitionSpec as P

MESH = pl.DeviceIdType.MESH
F32 = jnp.float32
BF16 = jnp.bfloat16
SCAN = 8


def one_minus_exp(y):
    series = 1.0 + y * (1.0 / 7.0)
    for n in (6.0, 5.0, 4.0, 3.0, 2.0):
        series = 1.0 + y * (1.0 / n) * series
    return jnp.where(y > -0.3, -y * series, 1.0 - jnp.exp(y))


def kernel(
    dims,
    res_hbm, gate_hbm, value_hbm, conv_ref, rate_ref, inp_ref, decay_ref, step_hbm,
    outw_hbm, gain_ref, up_hbm, down_hbm,
    out_ref,
    up_all, down_all, acc, act, normed, part, part_in, fin, fin_in,
    keep, drive, pad, gated, gate_v, value_v, step_v, outw_v, res_v, halo, tot, ent,
    upd, wpair, send, recv, tsend, trecv, csend, crecv, local_sem,
):
    n_sp, n_tp, ids = dims
    me, tp = lax.axis_index("sp"), lax.axis_index("tp")
    high = n_sp // 2
    hi, lo = me // 2, lax.rem(me, 2)
    rows, ch = value_v.shape
    width = up_all.shape[0]
    hidden = up_all.shape[1]
    piece = up_hbm.shape[0]
    own = rows // n_tp
    last = high // 2

    def at(step, side):
        low = lo if side == "o" else 1 - lo
        return lax.rem(hi + step + 2 * high, high) * 2 + low

    beside, above, below = at(0, "x"), at(1, "o"), at(-1, "o")

    loads = {}
    for n, (key, src, dst) in enumerate(
        (
            ("value", value_hbm, value_v),
            ("step", step_hbm, step_v),
            ("gate", gate_hbm, gate_v),
            ("outw", outw_hbm, outw_v),
            ("res", res_hbm.at[pl.ds(pl.multiple_of(tp * own, own), own), :], res_v),
            ("up", up_hbm, up_all.at[pl.ds(pl.multiple_of(me * piece, piece), piece), :]),
            ("down", down_hbm, down_all.at[pl.ds(pl.multiple_of(me * piece, piece), piece), :]),
        )
    ):
        loads[key] = pltpu.make_async_copy(src, dst, local_sem.at[n])
        loads[key].start()

    barrier = pltpu.get_barrier_semaphore()
    for d in range(1, n_sp):
        pl.semaphore_signal(
            barrier, inc=1, device_id=(lax.rem(me + d, n_sp), tp), device_id_type=MESH
        )
    for d in range(1, n_tp):
        pl.semaphore_signal(
            barrier, inc=1, device_id=(me, lax.rem(tp + d, n_tp)), device_id_type=MESH
        )
    pl.semaphore_wait(barrier, n_sp + n_tp - 2)

    started = {}

    def launch(key, src, dst, target):
        copy = pltpu.make_async_remote_copy(
            src_ref=src, dst_ref=dst, send_sem=send.at[ids[key]], recv_sem=recv.at[ids[key]],
            device_id=target, device_id_type=MESH,
        )
        copy.start()
        started[key] = copy

    def rows_of(ref, source, half):
        if half is None:
            return ref.at[pl.ds(pl.multiple_of(source * piece, piece), piece), :]
        h = piece // 2
        return ref.at[pl.ds(pl.multiple_of(source * piece + half * h, h), h), :]

    def half_of(k, sign):
        return None if k < last else (0 if sign > 0 else 1)

    def ring(name, hbm, buf, side, k, sign):
        source = at(-sign * (k - 1), side)
        half = half_of(k, sign)
        dst = rows_of(buf, source, half)
        if k == 1 and side == "o":
            h = piece // 2
            src = hbm if half is None else hbm.at[pl.ds(half * h, h), :]
        else:
            src = dst
        launch((name, side, k, sign), src, dst, (above if sign > 0 else below, tp))

    def ring_all(name, hbm, buf, side, k):
        for sign in (1, -1):
            ring(name, hbm, buf, side, k, sign)

    up_x_key, down_x_key = ("ux",), ("dx",)
    halo_copy_key = ("halo",)
    launch(
        halo_copy_key, value_hbm.at[pl.ds(rows - 16, 16), :], halo,
        (lax.rem(me + 1, n_sp), tp),
    )
    ring_all("u", up_hbm, up_all, "o", 1)
    launch(up_x_key, up_hbm, rows_of(up_all, me, None), (beside, tp))
    ring_all("d", down_hbm, down_all, "o", 1)
    launch(down_x_key, down_hbm, rows_of(down_all, me, None), (beside, tp))

    def up_forward(side, k):
        for sign in (1, -1):
            started[("u", side, k, sign)].wait_recv()
            if k < last:
                ring("u", up_hbm, up_all, side, k + 1, sign)

    def down_forward(k):
        for sign in (1, -1):
            started[("d", "o", k, sign)].wait_recv()
            if k < last:
                ring("d", down_hbm, down_all, "o", k + 1, sign)
        for sign in (1, -1):
            view = rows_of(down_all, at(-sign * k, "o"), half_of(k, sign))
            launch(("f", k, sign), view, view, (beside, tp))

    bw = rate_ref.shape[1]
    per = 128 // bw
    groups = ch // 128
    r_i = lax.broadcasted_iota(jnp.int32, (bw, 128), 0)
    c_i = lax.broadcasted_iota(jnp.int32, (bw, 128), 1)
    for g in range(groups):
        for which, ref in ((0, rate_ref), (1, inp_ref)):
            for j in range(per):
                place = jnp.where(c_i == r_i + j * bw, 1.0, 0.0).astype(BF16)
                block = jnp.dot(ref[g * per + j], place, preferred_element_type=F32)
                wpair[which, g, j * bw : (j + 1) * bw, :] = block.astype(BF16)

    loads["value"].wait()
    loads["step"].wait()
    started[halo_copy_key].wait_recv()
    taps = conv_ref.shape[0]
    first = jnp.where(me == 0, 0.0, 1.0).astype(F32)
    pad[0:8, :] = halo[8:16, :].astype(F32) * first

    chunk = 64

    def widen(r, c):
        at_row = pl.multiple_of(r * chunk, chunk)
        pad[pl.ds(pl.multiple_of(at_row + 8, 8), chunk), :] = value_v[
            pl.ds(at_row, chunk), :
        ].astype(F32)
        return c

    lax.fori_loop(0, rows // chunk, widen, 0)

    def gates(r, c):
        at_row = pl.multiple_of(r * chunk, chunk)
        for g in range(groups):
            lanes = slice(g * 128, (g + 1) * 128)
            window = pad[pl.ds(at_row, chunk + 8), lanes]
            total = jnp.zeros((chunk, 128), F32)
            for k in range(taps):
                shift = 8 - taps + 1 + k
                moved = window if shift == 0 else pltpu.roll(window, chunk + 8 - shift, 0)
                total = total + moved[0:chunk, :] * conv_ref[k : k + 1, lanes]
            smooth = total.astype(BF16)
            rate = lax.logistic(jnp.dot(smooth, wpair[0, g], preferred_element_type=F32))
            gate = lax.logistic(jnp.dot(smooth, wpair[1, g], preferred_element_type=F32))
            log_keep = -8.0 * step_v[pl.ds(at_row, chunk), lanes] * rate * decay_ref[0:1, lanes]
            keep[g, pl.ds(at_row, chunk), :] = jnp.exp(log_keep)
            drive[g, pl.ds(at_row, chunk), :] = (
                jnp.sqrt(one_minus_exp(2.0 * log_keep)) * gate * smooth.astype(F32)
            )
        return c

    lax.fori_loop(0, rows // chunk, gates, 0)

    seg = rows // SCAN

    def scan(i, carry):
        p, h = carry
        idx = pl.ds(i, SCAN, stride=seg)
        new_p, new_h = [], []
        for g in range(groups):
            a, d = keep[g, idx, :], drive[g, idx, :]
            hg = a * h[g] + d
            pg = a * p[g]
            keep[g, idx, :] = pg
            drive[g, idx, :] = hg
            new_p.append(pg)
            new_h.append(hg)
        return tuple(new_p), tuple(new_h)

    ones = tuple(jnp.ones((SCAN, 128), F32) for _ in range(groups))
    zeros = tuple(jnp.zeros((SCAN, 128), F32) for _ in range(groups))
    lax.fori_loop(0, seg, scan, (ones, zeros))

    def line(ref, row):
        return jnp.concatenate([ref[g, row : row + 1, :] for g in range(groups)], axis=1)

    ends = [(line(keep, (b + 1) * seg - 1), line(drive, (b + 1) * seg - 1)) for b in range(SCAN)]
    whole_p, whole_h = ends[0]
    for p_b, h_b in ends[1:]:
        whole_p, whole_h = whole_p * p_b, p_b * whole_h + h_b
    row_id = lax.broadcasted_iota(jnp.int32, (8, ch), 0)
    tot[me] = jnp.where(row_id == 0, whole_p, whole_h)
    carries = []
    for d in range(1, n_sp):
        copy = pltpu.make_async_remote_copy(
            src_ref=tot.at[me], dst_ref=tot.at[me], send_sem=csend.at[d], recv_sem=crecv.at[d],
            device_id=(lax.rem(me + d, n_sp), tp), device_id_type=MESH,
        )
        copy.start()
        carries.append(copy)
    loads["gate"].wait()
    loads["outw"].wait()
    for copy in carries:
        copy.wait_recv()

    def fold(d, s):
        joined = tot[d, 0:1, :] * s + tot[d, 1:2, :]
        return jnp.where(d < me, joined, s)

    state = lax.fori_loop(0, n_sp, fold, jnp.zeros((1, ch), F32))
    for b in range(SCAN):
        ent[b, 0:1, :] = state
        state = ends[b][0] * state + ends[b][1]

    def gating(b, c):
        at_row = pl.ds(pl.multiple_of(b * seg, seg), seg)
        for g in range(groups):
            lanes = slice(g * 128, (g + 1) * 128)
            full = drive[g, at_row, :] + keep[g, at_row, :] * ent[b, 0:1, lanes]
            branch = jax.nn.gelu(gate_v[at_row, lanes].astype(F32), approximate=True)
            gated[at_row, lanes] = (branch * full).astype(BF16)
        return c

    lax.fori_loop(0, SCAN, gating, 0)

    sums = []
    for d in list(range(1, n_tp)) + [0]:
        peer = lax.rem(tp + d, n_tp)
        span = pl.ds(pl.multiple_of(peer * own, own), own)
        part[span, :] = jnp.dot(gated[span, :], outw_v[...], preferred_element_type=F32).astype(BF16)
        if d:
            copy = pltpu.make_async_remote_copy(
                src_ref=part.at[span, :], dst_ref=part_in.at[tp],
                send_sem=tsend.at[0, d], recv_sem=trecv.at[0, d],
                device_id=(me, peer), device_id_type=MESH,
            )
            copy.start()
            sums.append(copy)

    started[up_x_key].wait_recv()
    ring_all("u", up_hbm, up_all, "x", 1)
    up_forward("o", 1)

    mine = pl.ds(pl.multiple_of(tp * own, own), own)
    loads["res"].wait()
    for copy in sums:
        copy.wait_recv()
    slab = 32

    def settle(r, c):
        here = pl.ds(pl.multiple_of(r * slab, slab), slab)
        there = pl.ds(pl.multiple_of(tp * own + r * slab, slab), slab)
        mixed = part[there, :].astype(F32)
        for d in range(1, n_tp):
            mixed = mixed + part_in[lax.rem(tp + d, n_tp), here, :].astype(F32)
        new = (res_v[here, :].astype(F32) + mixed).astype(BF16)
        upd[here, :] = new
        wide = new.astype(F32)
        factor = lax.rsqrt(jnp.mean(wide * wide, axis=-1, keepdims=True) + 1e-06)
        normed[there, :] = (wide * factor * gain_ref[0:1, :]).astype(BF16)
        return c

    lax.fori_loop(0, own // slab, settle, 0)
    shares = []
    for d in range(1, n_tp):
        copy = pltpu.make_async_remote_copy(
            src_ref=normed.at[mine, :], dst_ref=normed.at[mine, :],
            send_sem=tsend.at[1, d], recv_sem=trecv.at[1, d],
            device_id=(me, lax.rem(tp + d, n_tp)), device_id_type=MESH,
        )
        copy.start()
        shares.append(copy)

    down_forward(1)
    up_forward("x", 1)
    for k in range(2, last):
        up_forward("o", k)
        down_forward(k)
        up_forward("x", k)
    for copy in shares:
        copy.wait_recv()
    loads["up"].wait()
    loads["down"].wait()

    streaming = piece % 128 == 0
    tile = 512
    tiles = hidden // tile

    def gather_dot(sources, cols):
        total = None
        for s in sources:
            deep = pl.ds(pl.multiple_of(s * piece, piece), piece)
            term = jnp.dot(normed[:, deep], up_all[deep, cols], preferred_element_type=F32)
            total = term if total is None else total + term
        return total

    if streaming:
        early = [at(0, "o"), at(0, "x")]
        for k in range(1, last):
            early += [at(s, side) for s in (k, -k) for side in ("o", "x")]

        def early_tile(n, c):
            cols = pl.ds(pl.multiple_of(n * tile, tile), tile)
            acc[:, cols] = gather_dot(early, cols)
            return c

        lax.fori_loop(0, tiles, early_tile, 0)

    up_forward("o", last)
    down_forward(last)
    up_forward("x", last)

    def late_tile(n, c):
        cols = pl.ds(pl.multiple_of(n * tile, tile), tile)
        if streaming:
            lifted = acc[:, cols] + gather_dot([at(last, "o"), at(last, "x")], cols)
        else:
            lifted = jnp.dot(normed[...], up_all[:, cols], preferred_element_type=F32)
        lifted = jnp.maximum(lifted, 0.0)
        act[:, cols] = (lifted * lifted).astype(BF16)
        return c

    lax.fori_loop(0, tiles, late_tile, 0)

    def lower(start, size):
        cols = pl.ds(pl.multiple_of(start, size), size)
        fin[:, cols] = lax.dot_general(
            act[...], down_all[cols, :], (((1,), (1,)), ((), ())), preferred_element_type=F32
        ).astype(BF16)
        for d in range(1, n_tp):
            peer = lax.rem(tp + d, n_tp)
            pltpu.make_async_remote_copy(
                src_ref=fin.at[pl.ds(pl.multiple_of(peer * own, own), own), cols],
                dst_ref=fin_in.at[tp, :, cols],
                send_sem=tsend.at[2, d], recv_sem=trecv.at[2, d],
                device_id=(me, peer), device_id_type=MESH,
            ).start()

    def take(key):
        started[key].wait_recv()

    if streaming:
        lower(me * piece, piece)
        for k in range(1, last):
            for sign in (1, -1):
                lower(at(-sign * k, "o") * piece, piece)
        lower(at(last, "o") * piece, piece)
        take(down_x_key)
        lower(beside * piece, piece)
        for k in range(1, last):
            for sign in (1, -1):
                take(("f", k, sign))
                lower(at(-sign * k, "x") * piece, piece)
        for sign in (1, -1):
            take(("f", last, sign))
        lower(at(last, "x") * piece, piece)
    else:
        take(down_x_key)
        for k in range(1, last + 1):
            for sign in (1, -1):
                take(("f", k, sign))

        def block(b, c):
            lower(b * 256, 256)
            return c

        lax.fori_loop(0, width // 256, block, 0)

    for d in range(1, n_tp):
        peer = lax.rem(tp + d, n_tp)
        whole = pltpu.make_async_remote_copy(
            src_ref=fin.at[pl.ds(pl.multiple_of(peer * own, own), own), :],
            dst_ref=fin_in.at[lax.rem(tp - d + n_tp, n_tp)],
            send_sem=tsend.at[2, d], recv_sem=trecv.at[2, d],
            device_id=(me, peer), device_id_type=MESH,
        )
        whole.wait_recv()
        whole.wait_send()

    def finish(r, c):
        here = pl.ds(pl.multiple_of(r * slab, slab), slab)
        there = pl.ds(pl.multiple_of(tp * own + r * slab, slab), slab)
        total = fin[there, :].astype(F32)
        for d in range(1, n_tp):
            total = total + fin_in[lax.rem(tp + d, n_tp), here, :].astype(F32)
        out_ref[here, :] = (upd[here, :].astype(F32) + total).astype(BF16)
        return c

    lax.fori_loop(0, own // slab, finish, 0)
    for copy in list(started.values()) + carries + sums + shares:
        copy.wait_send()


def copy_ids(n_sp):
    last = n_sp // 4
    keys = [("ux",), ("dx",), ("halo",)]
    for k in range(1, last + 1):
        for sign in (1, -1):
            keys += [("u", "o", k, sign), ("u", "x", k, sign), ("d", "o", k, sign), ("f", k, sign)]
    return {key: n for n, key in enumerate(keys)}


def solution(mesh):
    n_sp, n_tp = mesh.shape["sp"], mesh.shape["tp"]
    ids = copy_ids(n_sp)

    def local(res, gate, value, conv, rate, inp, decay, step, outw, gain, up, down):
        rows, ch = value.shape
        width, hidden = outw.shape[1], up.shape[1]
        own = rows // n_tp
        V = pltpu.VMEM
        any_spec = pl.BlockSpec(memory_space=pl.ANY)
        vm = pl.BlockSpec(memory_space=pltpu.VMEM)
        dma = pltpu.SemaphoreType.DMA
        return pl.pallas_call(
            functools.partial(kernel, (n_sp, n_tp, ids)),
            out_shape=jax.ShapeDtypeStruct((own, width), BF16),
            in_specs=[any_spec, any_spec, any_spec, vm, vm, vm, vm, any_spec, any_spec, vm,
                      any_spec, any_spec],
            out_specs=vm,
            scratch_shapes=[
                V((width, hidden), BF16), V((width, hidden), BF16),
                V((rows, hidden), F32), V((rows, hidden), BF16), V((rows, width), BF16),
                V((rows, width), BF16), V((n_tp, own, width), BF16),
                V((rows, width), BF16), V((n_tp, own, width), BF16),
                V((ch // 128, rows, 128), F32), V((ch // 128, rows, 128), F32), V((rows + 8, ch), F32),
                V((rows, ch), BF16), V((rows, ch), BF16), V((rows, ch), BF16),
                V((rows, ch), F32), V((ch, width), BF16), V((own, width), BF16),
                V((16, ch), BF16), V((n_sp, 8, ch), F32), V((SCAN, 8, ch), F32),
                V((own, width), BF16), V((2, ch // 128, 128, 128), BF16),
                dma((len(ids),)), dma((len(ids),)), dma((3, n_tp)), dma((3, n_tp)),
                dma((n_sp,)), dma((n_sp,)), dma((7,)),
            ],
            compiler_params=pltpu.CompilerParams(
                collective_id=0, has_side_effects=True, vmem_limit_bytes=62 * 1024 * 1024
            ),
        )(res, gate, value, conv, rate, inp, decay.reshape(1, -1), step, outw,
          gain.reshape(1, -1), up, down)

    in_specs = (
        P("sp", None), P("sp", "tp"), P("sp", "tp"), P(None, "tp"),
        P("tp", None, None), P("tp", None, None), P("tp"), P("sp", "tp"),
        P("tp", None), P(), P("sp", "tp"), P("sp", "tp"),
    )
    return jax.shard_map(
        local, mesh=mesh, in_specs=in_specs, out_specs=P(("sp", "tp"), None), check_vma=False
    )
```

time: 489 us -> 247 us (0.51)
  waiting for transfers between devices: 273 us -> 0 us
  Pallas kernels: 0 us -> 245 us
  local copies, waits for them, and re-layouts: 104 us -> 1.88 us
  blocking collectives: 52.7 us -> 0 us
  matrix products: 20.2 us -> 0 us
  other arithmetic: 15.8 us -> 0 us
  between operations: 15.3 us -> 0.01 us
  starting transfers between devices: 5.19 us -> 0 us
    pallas_call x0 -> x1, Pallas kernels: none -> 245 us  [local(): pl.pallas_call(functools.partial(kernel, (n_sp, n_tp, ids)), out_shape=ja...]
    all_gather x2 -> x0, waiting for transfers between devices: 195 us -> none  [the longest x1 124 us: local(): lax.all_gather(down_weight, 'sp', axis=0, tiled=True)]
    dynamic_update_slice x64 -> x0, local copies, waits for them, and re-layouts: 70.1 us -> none  [local(): lax.scan(step_rows, start_carry, (keep_blocks, drive_blocks))]
    all_gather x2 -> x0, blocking collectives: 52.7 us -> none  [carried_in(): gathered = jax.tree.map(lambda a: lax.all_gather(a, axis), part)]
    psum x1 -> x0, waiting for transfers between devices: 47.5 us -> none  [local(): lax.psum(rounded(jnp.dot(gated, out_weight, preferred_element_type=jnp.fl...]
    reduce_scatter x1 -> x0, waiting for transfers between devices: 29.5 us -> none  [local(): lax.psum_scatter(rounded(partial_rows).astype(jnp.bfloat16), 'tp', scatte...]
    dynamic_slice x16 -> x0, local copies, waits for them, and re-layouts: 21 us -> none  [local(): lax.scan(step_rows, start_carry, (keep_blocks, drive_blocks))]
    dot_general x4 -> x0, matrix products: 20.2 us -> none  [the longest x1 16.6 us: local(): lax.dot_general(activated, lax.all_gather(down_weight, 'sp', axis=0, tile...]
  transfers between devices with their start and end apart: 5 -> 0, of which waited for: 4 -> 0; matrix products, arithmetic and copies ran while one was open for 2% -> 0% of each run, Pallas kernels for 0% -> 0%
where the time goes in v1:
time: 247 us
  Pallas kernels  245 us (99%)
    pallas_call x1, Pallas kernels, local(): pl.pallas_call(functools.partial(kernel, (n_sp, n_tp, ids)), out_shape=ja...  245 us

profile of v1, /device:TPU:0, one launch (start us, length us, event | category | flops | bytes accessed | tf_op | source)
XLA Modules:
  0.0 246.8 jit_solution(13531527947097307126)
XLA Ops:
  0.0 244.9 %shard_map.118 = bf16[128,2048]{1,0:T(8,128)(2,1)} custom-call(bf16[512,2048]{1,0:T(8,128)(2,1)} %res_hbm.1, bf16[512,512]{1,0:T(8,128)(2,1)} %gate_hbm.1, bf16[512,512]{1,0:T(8,128)(2,1)} %value_hbm.1, f32[4,512]{1,0:T(4,128)} %conv_ref.1, bf16[8,64,64]{2,1,0:T(8,128)(2,1)} %rate_ref.1, bf16[8,64,64]{2,1,0:T(8,128)(2,1)} %inp_ref.1, f32[1,512]{1,0:T(1,128)} %bitcast.3, ...), custom_call_target="tpu_custom_call" | custom-call | tf_op jit(solution)/shard_map/pallas_call | solution.py:438
  244.9 1.9 copy.14

commit v2 on v1

--- a/solution.py
+++ b/solution.py
@@ -25,7 +25,7 @@
     res_hbm, gate_hbm, value_hbm, conv_ref, rate_ref, inp_ref, decay_ref, step_hbm,
     outw_hbm, gain_ref, up_hbm, down_hbm,
     out_ref,
-    up_all, down_all, acc, act, normed, part, part_in, fin, fin_in,
+    up_all, down_all, act, normed, part, part_in, fin, fin_in,
     keep, drive, pad, gated, gate_v, value_v, step_v, outw_v, res_v, halo, tot, ent,
     upd, wpair, send, recv, tsend, trecv, csend, crecv, local_sem,
 ):
@@ -38,7 +38,6 @@
     hidden = up_all.shape[1]
     piece = up_hbm.shape[0]
     own = rows // n_tp
-    last = high // 2
 
     def at(step, side):
         low = lo if side == "o" else 1 - lo
@@ -74,63 +73,74 @@
 
     started = {}
 
-    def launch(key, src, dst, target):
+    def guarded(cond, act_on):
+        if cond is None:
+            act_on()
+        else:
+            pl.when(cond)(act_on)
+
+    def launch(key, src, dst, target, send_if=None, recv_if=None):
         copy = pltpu.make_async_remote_copy(
             src_ref=src, dst_ref=dst, send_sem=send.at[ids[key]], recv_sem=recv.at[ids[key]],
             device_id=target, device_id_type=MESH,
         )
-        copy.start()
-        started[key] = copy
-
-    def rows_of(ref, source, half):
-        if half is None:
-            return ref.at[pl.ds(pl.multiple_of(source * piece, piece), piece), :]
-        h = piece // 2
-        return ref.at[pl.ds(pl.multiple_of(source * piece + half * h, h), h), :]
-
-    def half_of(k, sign):
-        return None if k < last else (0 if sign > 0 else 1)
-
-    def ring(name, hbm, buf, side, k, sign):
-        source = at(-sign * (k - 1), side)
-        half = half_of(k, sign)
-        dst = rows_of(buf, source, half)
-        if k == 1 and side == "o":
-            h = piece // 2
-            src = hbm if half is None else hbm.at[pl.ds(half * h, h), :]
-        else:
-            src = dst
-        launch((name, side, k, sign), src, dst, (above if sign > 0 else below, tp))
-
-    def ring_all(name, hbm, buf, side, k):
+        guarded(send_if, copy.start)
+        started[key] = (copy, send_if, recv_if)
+
+    def take(key):
+        copy, _, recv_if = started[key]
+        guarded(recv_if, copy.wait_recv)
+
+    split = max(16, piece * 3 // 8 // 16 * 16)
+    streams = {
+        "a": (up_hbm, 0, split, up_all),
+        "b": (up_hbm, split, piece - split, up_all),
+        "c": (down_hbm, 0, piece, down_all),
+    }
+
+    def landed(name, source):
+        _, start, size, buf = streams[name]
+        return buf.at[pl.ds(pl.multiple_of(source * piece + start, 16), size), :]
+
+    def origin(name):
+        hbm, start, size, _ = streams[name]
+        return hbm.at[pl.ds(start, size), :]
+
+    def has(k, sign):
+        return hi >= k if sign > 0 else hi + k < high
+
+    def line(name, side, k):
         for sign in (1, -1):
-            ring(name, hbm, buf, side, k, sign)
-
-    up_x_key, down_x_key = ("ux",), ("dx",)
+            source = at(-sign * (k - 1), side)
+            dst = landed(name, source)
+            src = origin(name) if k == 1 and side == "o" else dst
+            onward = hi + 1 < high if sign > 0 else hi >= 1
+            send_if = onward if k == 1 else jnp.logical_and(onward, has(k - 1, sign))
+            launch((name, side, k, sign), src, dst, (above if sign > 0 else below, tp),
+                   send_if, has(k, sign))
+
+    def across(name):
+        launch((name, "x"), origin(name), landed(name, me), (beside, tp))
+
+    def forward(name, side, k):
+        for sign in (1, -1):
+            take((name, side, k, sign))
+        if k < high - 1:
+            line(name, side, k + 1)
+        if name != "a":
+            for sign in (1, -1):
+                view = landed(name, at(-sign * k, "o"))
+                launch((name, "f", k, sign), view, view, (beside, tp), has(k, sign), has(k, sign))
+
     halo_copy_key = ("halo",)
     launch(
         halo_copy_key, value_hbm.at[pl.ds(rows - 16, 16), :], halo,
         (lax.rem(me + 1, n_sp), tp),
     )
-    ring_all("u", up_hbm, up_all, "o", 1)
-    launch(up_x_key, up_hbm, rows_of(up_all, me, None), (beside, tp))
-    ring_all("d", down_hbm, down_all, "o", 1)
-    launch(down_x_key, down_hbm, rows_of(down_all, me, None), (beside, tp))
-
-    def up_forward(side, k):
-        for sign in (1, -1):
-            started[("u", side, k, sign)].wait_recv()
-            if k < last:
-                ring("u", up_hbm, up_all, side, k + 1, sign)
-
-    def down_forward(k):
-        for sign in (1, -1):
-            started[("d", "o", k, sign)].wait_recv()
-            if k < last:
-                ring("d", down_hbm, down_all, "o", k + 1, sign)
-        for sign in (1, -1):
-            view = rows_of(down_all, at(-sign * k, "o"), half_of(k, sign))
-            launch(("f", k, sign), view, view, (beside, tp))
+    line("a", "o", 1)
+    line("b", "o", 1)
+    across("a")
+    across("b")
 
     bw = rate_ref.shape[1]
     per = 128 // bw
@@ -146,7 +156,7 @@
 
     loads["value"].wait()
     loads["step"].wait()
-    started[halo_copy_key].wait_recv()
+    take(halo_copy_key)
     taps = conv_ref.shape[0]
     first = jnp.where(me == 0, 0.0, 1.0).astype(F32)
     pad[0:8, :] = halo[8:16, :].astype(F32) * first
@@ -204,10 +214,10 @@
     zeros = tuple(jnp.zeros((SCAN, 128), F32) for _ in range(groups))
     lax.fori_loop(0, seg, scan, (ones, zeros))
 
-    def line(ref, row):
+    def pick(ref, row):
         return jnp.concatenate([ref[g, row : row + 1, :] for g in range(groups)], axis=1)
 
-    ends = [(line(keep, (b + 1) * seg - 1), line(drive, (b + 1) * seg - 1)) for b in range(SCAN)]
+    ends = [(pick(keep, (b + 1) * seg - 1), pick(drive, (b + 1) * seg - 1)) for b in range(SCAN)]
     whole_p, whole_h = ends[0]
     for p_b, h_b in ends[1:]:
         whole_p, whole_h = whole_p * p_b, p_b * whole_h + h_b
@@ -260,9 +270,12 @@
             copy.start()
             sums.append(copy)
 
-    started[up_x_key].wait_recv()
-    ring_all("u", up_hbm, up_all, "x", 1)
-    up_forward("o", 1)
+    forward("a", "o", 1)
+    forward("b", "o", 1)
+    take(("a", "x"))
+    line("a", "x", 1)
+    line("c", "o", 1)
+    across("c")
 
     mine = pl.ds(pl.multiple_of(tp * own, own), own)
     loads["res"].wait()
@@ -294,12 +307,12 @@
         copy.start()
         shares.append(copy)
 
-    down_forward(1)
-    up_forward("x", 1)
-    for k in range(2, last):
-        up_forward("o", k)
-        down_forward(k)
-        up_forward("x", k)
+    for k in range(2, high):
+        forward("b", "o", k)
+        forward("a", "o", k)
+        forward("a", "x", k - 1)
+        forward("c", "o", k - 1)
+    forward("a", "x", high - 1)
     for copy in shares:
         copy.wait_recv()
     loads["up"].wait()
@@ -309,36 +322,14 @@
     tile = 512
     tiles = hidden // tile
 
-    def gather_dot(sources, cols):
-        total = None
-        for s in sources:
-            deep = pl.ds(pl.multiple_of(s * piece, piece), piece)
-            term = jnp.dot(normed[:, deep], up_all[deep, cols], preferred_element_type=F32)
-            total = term if total is None else total + term
-        return total
-
-    if streaming:
-        early = [at(0, "o"), at(0, "x")]
-        for k in range(1, last):
-            early += [at(s, side) for s in (k, -k) for side in ("o", "x")]
-
-        def early_tile(n, c):
-            cols = pl.ds(pl.multiple_of(n * tile, tile), tile)
-            acc[:, cols] = gather_dot(early, cols)
-            return c
-
-        lax.fori_loop(0, tiles, early_tile, 0)
-
-    up_forward("o", last)
-    down_forward(last)
-    up_forward("x", last)
+    take(("b", "x"))
+    for k in range(1, high):
+        for sign in (1, -1):
+            take(("b", "f", k, sign))
 
     def late_tile(n, c):
         cols = pl.ds(pl.multiple_of(n * tile, tile), tile)
-        if streaming:
-            lifted = acc[:, cols] + gather_dot([at(last, "o"), at(last, "x")], cols)
-        else:
-            lifted = jnp.dot(normed[...], up_all[:, cols], preferred_element_type=F32)
+        lifted = jnp.dot(normed[...], up_all[:, cols], preferred_element_type=F32)
         lifted = jnp.maximum(lifted, 0.0)
         act[:, cols] = (lifted * lifted).astype(BF16)
         return c
@@ -359,29 +350,28 @@
                 device_id=(me, peer), device_id_type=MESH,
             ).start()
 
-    def take(key):
-        started[key].wait_recv()
-
     if streaming:
+        def lower_if(k, sign, side):
+            pl.when(has(k, sign))(lambda: lower(at(-sign * k, side) * piece, piece))
+
         lower(me * piece, piece)
-        for k in range(1, last):
+        for k in range(1, high):
+            if k == high - 1:
+                forward("c", "o", k)
             for sign in (1, -1):
-                lower(at(-sign * k, "o") * piece, piece)
-        lower(at(last, "o") * piece, piece)
-        take(down_x_key)
+                lower_if(k, sign, "o")
+        take(("c", "x"))
         lower(beside * piece, piece)
-        for k in range(1, last):
+        for k in range(1, high):
             for sign in (1, -1):
-                take(("f", k, sign))
-                lower(at(-sign * k, "x") * piece, piece)
-        for sign in (1, -1):
-            take(("f", last, sign))
-        lower(at(last, "x") * piece, piece)
+                take(("c", "f", k, sign))
+                lower_if(k, sign, "x")
     else:
-        take(down_x_key)
-        for k in range(1, last + 1):
+        forward("c", "o", high - 1)
+        take(("c", "x"))
+        for k in range(1, high):
             for sign in (1, -1):
-                take(("f", k, sign))
+                take(("c", "f", k, sign))
 
         def block(b, c):
             lower(b * 256, 256)
@@ -410,16 +400,18 @@
         return c
 
     lax.fori_loop(0, own // slab, finish, 0)
-    for copy in list(started.values()) + carries + sums + shares:
+    for copy, send_if, _ in started.values():
+        guarded(send_if, copy.wait_send)
+    for copy in carries + sums + shares:
         copy.wait_send()
 
 
 def copy_ids(n_sp):
-    last = n_sp // 4
-    keys = [("ux",), ("dx",), ("halo",)]
-    for k in range(1, last + 1):
+    keys = [("a", "x"), ("b", "x"), ("c", "x"), ("halo",)]
+    for k in range(1, n_sp // 2):
         for sign in (1, -1):
-            keys += [("u", "o", k, sign), ("u", "x", k, sign), ("d", "o", k, sign), ("f", k, sign)]
+            keys += [(name, side, k, sign) for name, side in
+                     (("a", "o"), ("a", "x"), ("b", "o"), ("c", "o"), ("b", "f"), ("c", "f"))]
     return {key: n for n, key in enumerate(keys)}
 
 
@@ -443,7 +435,7 @@
             out_specs=vm,
             scratch_shapes=[
                 V((width, hidden), BF16), V((width, hidden), BF16),
-                V((rows, hidden), F32), V((rows, hidden), BF16), V((rows, width), BF16),
+                V((rows, hidden), BF16), V((rows, width), BF16),
                 V((rows, width), BF16), V((n_tp, own, width), BF16),
                 V((rows, width), BF16), V((n_tp, own, width), BF16),
                 V((ch // 128, rows, 128), F32), V((ch // 128, rows, 128), F32), V((rows + 8, ch), F32),

time: 247 us -> 205 us (0.83)
  Pallas kernels: 245 us -> 203 us
    pallas_call x1, Pallas kernels: 245 us -> 203 us  [local(): pl.pallas_call(functools.partial(kernel, (n_sp, n_tp, ids)), out_shape=ja...]
where the time goes in v2:
time: 205 us
  Pallas kernels  203 us (99%)
    pallas_call x1, Pallas kernels, local(): pl.pallas_call(functools.partial(kernel, (n_sp, n_tp, ids)), out_shape=ja...  203 us

profile of v2, /device:TPU:0, one launch (start us, length us, event | category | flops | bytes accessed | tf_op | source)
XLA Modules:
  0.0 204.5 jit_solution(1980170685169892647)
XLA Ops:
  0.0 202.6 %shard_map.118 = bf16[128,2048]{1,0:T(8,128)(2,1)} custom-call(bf16[512,2048]{1,0:T(8,128)(2,1)} %res_hbm.1, bf16[512,512]{1,0:T(8,128)(2,1)} %gate_hbm.1, bf16[512,512]{1,0:T(8,128)(2,1)} %value_hbm.1, f32[4,512]{1,0:T(4,128)} %conv_ref.1, bf16[8,64,64]{2,1,0:T(8,128)(2,1)} %rate_ref.1, bf16[8,64,64]{2,1,0:T(8,128)(2,1)} %inp_ref.1, f32[1,512]{1,0:T(1,128)} %bitcast.3, ...), custom_call_target="tpu_custom_call" | custom-call | tf_op jit(solution)/shard_map/pallas_call | solution.py:430
  202.6 1.9 copy.14

commit v3 on v2

--- a/solution.py
+++ b/solution.py
@@ -25,14 +25,17 @@
     res_hbm, gate_hbm, value_hbm, conv_ref, rate_ref, inp_ref, decay_ref, step_hbm,
     outw_hbm, gain_ref, up_hbm, down_hbm,
     out_ref,
-    up_all, down_all, act, normed, part, part_in, fin, fin_in,
+    up_all, down_all, act, normed, part, part_in, fin, fin_in, far_out, far_in,
     keep, drive, pad, gated, gate_v, value_v, step_v, outw_v, res_v, halo, tot, ent,
-    upd, wpair, send, recv, tsend, trecv, csend, crecv, local_sem,
+    upd, wpair, send, recv, tsend, trecv, fsend, frecv, csend, crecv, local_sem,
 ):
     n_sp, n_tp, ids = dims
     me, tp = lax.axis_index("sp"), lax.axis_index("tp")
-    high = n_sp // 2
-    hi, lo = me // 2, lax.rem(me, 2)
+    half_size = n_sp // 2
+    high = half_size // 2
+    half, place_in = me // half_size, lax.rem(me, half_size)
+    hi, lo = place_in // 2, lax.rem(place_in, 2)
+    partner = lax.rem(me + half_size, n_sp)
     rows, ch = value_v.shape
     width = up_all.shape[0]
     hidden = up_all.shape[1]
@@ -41,9 +44,12 @@
 
     def at(step, side):
         low = lo if side == "o" else 1 - lo
-        return lax.rem(hi + step + 2 * high, high) * 2 + low
+        return half * half_size + lax.rem(hi + step + 2 * high, high) * 2 + low
 
     beside, above, below = at(0, "x"), at(1, "o"), at(-1, "o")
+
+    kept = pl.ds(pl.multiple_of(half * hidden, 128), hidden)
+    given = pl.ds(pl.multiple_of((1 - half) * hidden, 128), hidden)
 
     loads = {}
     for n, (key, src, dst) in enumerate(
@@ -53,8 +59,8 @@
             ("gate", gate_hbm, gate_v),
             ("outw", outw_hbm, outw_v),
             ("res", res_hbm.at[pl.ds(pl.multiple_of(tp * own, own), own), :], res_v),
-            ("up", up_hbm, up_all.at[pl.ds(pl.multiple_of(me * piece, piece), piece), :]),
-            ("down", down_hbm, down_all.at[pl.ds(pl.multiple_of(me * piece, piece), piece), :]),
+            ("up", up_hbm.at[:, kept], up_all.at[pl.ds(pl.multiple_of(me * piece, piece), piece), :]),
+            ("down", down_hbm.at[:, kept], down_all.at[pl.ds(pl.multiple_of(me * piece, piece), piece), :]),
         )
     ):
         loads[key] = pltpu.make_async_copy(src, dst, local_sem.at[n])
@@ -91,56 +97,60 @@
         copy, _, recv_if = started[key]
         guarded(recv_if, copy.wait_recv)
 
-    split = max(16, piece * 3 // 8 // 16 * 16)
     streams = {
-        "a": (up_hbm, 0, split, up_all),
-        "b": (up_hbm, split, piece - split, up_all),
-        "c": (down_hbm, 0, piece, down_all),
+        "u": (up_hbm, False, up_all),
+        "v": (up_hbm, True, up_all),
+        "c": (down_hbm, False, down_all),
+        "e": (down_hbm, True, down_all),
     }
 
     def landed(name, source):
-        _, start, size, buf = streams[name]
-        return buf.at[pl.ds(pl.multiple_of(source * piece + start, 16), size), :]
+        _, far, buf = streams[name]
+        if far:
+            source = lax.rem(source + half_size, n_sp)
+        return buf.at[pl.ds(pl.multiple_of(source * piece, 16), piece), :]
 
     def origin(name):
-        hbm, start, size, _ = streams[name]
-        return hbm.at[pl.ds(start, size), :]
+        hbm, far, _ = streams[name]
+        return landed(name, me) if far else hbm.at[:, kept]
 
     def has(k, sign):
         return hi >= k if sign > 0 else hi + k < high
 
-    def line(name, side, k):
+    def line(name, k):
         for sign in (1, -1):
-            source = at(-sign * (k - 1), side)
-            dst = landed(name, source)
-            src = origin(name) if k == 1 and side == "o" else dst
+            dst = landed(name, at(-sign * (k - 1), "o"))
+            src = origin(name) if k == 1 else dst
             onward = hi + 1 < high if sign > 0 else hi >= 1
             send_if = onward if k == 1 else jnp.logical_and(onward, has(k - 1, sign))
-            launch((name, side, k, sign), src, dst, (above if sign > 0 else below, tp),
+            launch((name, "o", k, sign), src, dst, (above if sign > 0 else below, tp),
                    send_if, has(k, sign))
 
     def across(name):
         launch((name, "x"), origin(name), landed(name, me), (beside, tp))
 
-    def forward(name, side, k):
+    def forward(name, k):
         for sign in (1, -1):
-            take((name, side, k, sign))
+            take((name, "o", k, sign))
         if k < high - 1:
-            line(name, side, k + 1)
-        if name != "a":
-            for sign in (1, -1):
-                view = landed(name, at(-sign * k, "o"))
-                launch((name, "f", k, sign), view, view, (beside, tp), has(k, sign), has(k, sign))
+            line(name, k + 1)
+        for sign in (1, -1):
+            view = landed(name, at(-sign * k, "o"))
+            launch((name, "f", k, sign), view, view, (beside, tp), has(k, sign), has(k, sign))
 
     halo_copy_key = ("halo",)
     launch(
         halo_copy_key, value_hbm.at[pl.ds(rows - 16, 16), :], halo,
         (lax.rem(me + 1, n_sp), tp),
     )
-    line("a", "o", 1)
-    line("b", "o", 1)
-    across("a")
-    across("b")
+    mine_up = up_all.at[pl.ds(pl.multiple_of(me * piece, 16), piece), :]
+    mine_down = down_all.at[pl.ds(pl.multiple_of(me * piece, 16), piece), :]
+    launch(("pu",), up_hbm.at[:, given], mine_up, (partner, tp))
+    line("u", 1)
+    across("u")
+    launch(("pd",), down_hbm.at[:, given], mine_down, (partner, tp))
+    line("c", 1)
+    across("c")
 
     bw = rate_ref.shape[1]
     per = 128 // bw
@@ -270,12 +280,10 @@
             copy.start()
             sums.append(copy)
 
-    forward("a", "o", 1)
-    forward("b", "o", 1)
-    take(("a", "x"))
-    line("a", "x", 1)
-    line("c", "o", 1)
-    across("c")
+    take(("pu",))
+    line("v", 1)
+    across("v")
+    forward("u", 1)
 
     mine = pl.ds(pl.multiple_of(tp * own, own), own)
     loads["res"].wait()
@@ -298,131 +306,148 @@
 
     lax.fori_loop(0, own // slab, settle, 0)
     shares = []
-    for d in range(1, n_tp):
-        copy = pltpu.make_async_remote_copy(
-            src_ref=normed.at[mine, :], dst_ref=normed.at[mine, :],
-            send_sem=tsend.at[1, d], recv_sem=trecv.at[1, d],
-            device_id=(me, lax.rem(tp + d, n_tp)), device_id_type=MESH,
-        )
-        copy.start()
-        shares.append(copy)
-
+    far_mine = pl.ds(pl.multiple_of(rows + tp * own, own), own)
+    launch(("n",), normed.at[mine, :], normed.at[far_mine, :], (partner, tp))
+
+    def share(span, turn):
+        copies = []
+        for d in range(1, n_tp):
+            copy = pltpu.make_async_remote_copy(
+                src_ref=normed.at[span, :], dst_ref=normed.at[span, :],
+                send_sem=tsend.at[turn, d], recv_sem=trecv.at[turn, d],
+                device_id=(me, lax.rem(tp + d, n_tp)), device_id_type=MESH,
+            )
+            copy.start()
+            copies.append(copy)
+        return copies
+
+    shares = share(mine, 1)
+    take(("pd",))
+    line("e", 1)
+    across("e")
+    forward("c", 1)
+    forward("v", 1)
+    take(("n",))
+    shares_far = share(far_mine, 2)
+    forward("e", 1)
     for k in range(2, high):
-        forward("b", "o", k)
-        forward("a", "o", k)
-        forward("a", "x", k - 1)
-        forward("c", "o", k - 1)
-    forward("a", "x", high - 1)
+        for name in ("u", "v", "c", "e"):
+            forward(name, k)
+    loads["up"].wait()
+    loads["down"].wait()
+
+    def settle_stream(name):
+        take((name, "x"))
+        for k in range(1, high):
+            for sign in (1, -1):
+                take((name, "f", k, sign))
+
+    settle_stream("u")
+    settle_stream("v")
+    tile = 512
+
     for copy in shares:
         copy.wait_recv()
-    loads["up"].wait()
-    loads["down"].wait()
-
-    streaming = piece % 128 == 0
-    tile = 512
-    tiles = hidden // tile
-
-    take(("b", "x"))
-    for k in range(1, high):
-        for sign in (1, -1):
-            take(("b", "f", k, sign))
-
-    def late_tile(n, c):
-        cols = pl.ds(pl.multiple_of(n * tile, tile), tile)
-        lifted = jnp.dot(normed[...], up_all[:, cols], preferred_element_type=F32)
-        lifted = jnp.maximum(lifted, 0.0)
-        act[:, cols] = (lifted * lifted).astype(BF16)
-        return c
-
-    lax.fori_loop(0, tiles, late_tile, 0)
-
-    def lower(start, size):
-        cols = pl.ds(pl.multiple_of(start, size), size)
-        fin[:, cols] = lax.dot_general(
-            act[...], down_all[cols, :], (((1,), (1,)), ((), ())), preferred_element_type=F32
+    def raise_rows(start):
+        def one(n, c):
+            cols = pl.ds(pl.multiple_of(n * tile, tile), tile)
+            lifted = jnp.dot(
+                normed[start : start + rows, :], up_all[:, cols], preferred_element_type=F32
+            )
+            lifted = jnp.maximum(lifted, 0.0)
+            act[start : start + rows, cols] = (lifted * lifted).astype(BF16)
+            return c
+
+        lax.fori_loop(0, hidden // tile, one, 0)
+
+    raise_rows(0)
+    for copy in shares_far:
+        copy.wait_recv()
+    raise_rows(rows)
+    settle_stream("c")
+    settle_stream("e")
+    blocks = width // tile
+    lowered = {}
+
+    def lower(side, q):
+        cols = slice(q * tile, (q + 1) * tile)
+        base = side * rows
+        fin[base : base + rows, cols] = lax.dot_general(
+            act[base : base + rows, :], down_all[cols, :], (((1,), (1,)), ((), ())),
+            preferred_element_type=F32,
         ).astype(BF16)
         for d in range(1, n_tp):
             peer = lax.rem(tp + d, n_tp)
-            pltpu.make_async_remote_copy(
-                src_ref=fin.at[pl.ds(pl.multiple_of(peer * own, own), own), cols],
-                dst_ref=fin_in.at[tp, :, cols],
-                send_sem=tsend.at[2, d], recv_sem=trecv.at[2, d],
+            copy = pltpu.make_async_remote_copy(
+                src_ref=fin.at[pl.ds(pl.multiple_of(base + peer * own, own), own), cols],
+                dst_ref=fin_in.at[tp, side * own : (side + 1) * own, cols],
+                send_sem=fsend.at[side * blocks + q, d], recv_sem=frecv.at[side * blocks + q, d],
                 device_id=(me, peer), device_id_type=MESH,
-            ).start()
-
-    if streaming:
-        def lower_if(k, sign, side):
-            pl.when(has(k, sign))(lambda: lower(at(-sign * k, side) * piece, piece))
-
-        lower(me * piece, piece)
-        for k in range(1, high):
-            if k == high - 1:
-                forward("c", "o", k)
-            for sign in (1, -1):
-                lower_if(k, sign, "o")
-        take(("c", "x"))
-        lower(beside * piece, piece)
-        for k in range(1, high):
-            for sign in (1, -1):
-                take(("c", "f", k, sign))
-                lower_if(k, sign, "x")
-    else:
-        forward("c", "o", high - 1)
-        take(("c", "x"))
-        for k in range(1, high):
-            for sign in (1, -1):
-                take(("c", "f", k, sign))
-
-        def block(b, c):
-            lower(b * 256, 256)
+            )
+            copy.start()
+            lowered[side, q, d] = copy
+
+    def gathered(side, r, cols):
+        here = pl.ds(pl.multiple_of(side * own + r * slab, slab), slab)
+        there = pl.ds(pl.multiple_of(side * rows + tp * own + r * slab, slab), slab)
+        total = fin[there, cols].astype(F32)
+        for d in range(1, n_tp):
+            total = total + fin_in[lax.rem(tp + d, n_tp), here, cols].astype(F32)
+        return total
+
+    for side in (1, 0):
+        for q in range(blocks):
+            lower(side, q)
+    for q in range(blocks):
+        cols = slice(q * tile, (q + 1) * tile)
+        for d in range(1, n_tp):
+            lowered[1, q, d].wait_recv()
+
+        def far_sum(r, c, cols=cols):
+            here = pl.ds(pl.multiple_of(r * slab, slab), slab)
+            far_out[here, cols] = gathered(1, r, cols).astype(BF16)
             return c
 
-        lax.fori_loop(0, width // 256, block, 0)
-
-    for d in range(1, n_tp):
-        peer = lax.rem(tp + d, n_tp)
-        whole = pltpu.make_async_remote_copy(
-            src_ref=fin.at[pl.ds(pl.multiple_of(peer * own, own), own), :],
-            dst_ref=fin_in.at[lax.rem(tp - d + n_tp, n_tp)],
-            send_sem=tsend.at[2, d], recv_sem=trecv.at[2, d],
-            device_id=(me, peer), device_id_type=MESH,
-        )
-        whole.wait_recv()
-        whole.wait_send()
-
-    def finish(r, c):
-        here = pl.ds(pl.multiple_of(r * slab, slab), slab)
-        there = pl.ds(pl.multiple_of(tp * own + r * slab, slab), slab)
-        total = fin[there, :].astype(F32)
-        for d in range(1, n_tp):
-            total = total + fin_in[lax.rem(tp + d, n_tp), here, :].astype(F32)
-        out_ref[here, :] = (upd[here, :].astype(F32) + total).astype(BF16)
-        return c
-
-    lax.fori_loop(0, own // slab, finish, 0)
+        lax.fori_loop(0, own // slab, far_sum, 0)
+        launch(("r", q), far_out.at[:, cols], far_in.at[:, cols], (partner, tp))
+    for q in range(blocks):
+        cols = slice(q * tile, (q + 1) * tile)
+        for d in range(1, n_tp):
+            lowered[0, q, d].wait_recv()
+        take(("r", q))
+
+        def finish(r, c, cols=cols):
+            here = pl.ds(pl.multiple_of(r * slab, slab), slab)
+            total = gathered(0, r, cols) + far_in[here, cols].astype(F32)
+            out_ref[here, cols] = (upd[here, cols].astype(F32) + total).astype(BF16)
+            return c
+
+        lax.fori_loop(0, own // slab, finish, 0)
     for copy, send_if, _ in started.values():
         guarded(send_if, copy.wait_send)
-    for copy in carries + sums + shares:
+    for copy in carries + sums + shares + shares_far + list(lowered.values()):
         copy.wait_send()
 
 
-def copy_ids(n_sp):
-    keys = [("a", "x"), ("b", "x"), ("c", "x"), ("halo",)]
-    for k in range(1, n_sp // 2):
-        for sign in (1, -1):
-            keys += [(name, side, k, sign) for name, side in
-                     (("a", "o"), ("a", "x"), ("b", "o"), ("c", "o"), ("b", "f"), ("c", "f"))]
+def copy_ids(n_sp, blocks):
+    keys = [("pu",), ("pd",), ("halo",), ("n",)] + [("r", q) for q in range(blocks)]
+    for name in ("u", "v", "c", "e"):
+        keys.append((name, "x"))
+        for k in range(1, n_sp // 4):
+            for sign in (1, -1):
+                keys += [(name, "o", k, sign), (name, "f", k, sign)]
     return {key: n for n, key in enumerate(keys)}
 
 
 def solution(mesh):
     n_sp, n_tp = mesh.shape["sp"], mesh.shape["tp"]
-    ids = copy_ids(n_sp)
 
     def local(res, gate, value, conv, rate, inp, decay, step, outw, gain, up, down):
         rows, ch = value.shape
         width, hidden = outw.shape[1], up.shape[1]
         own = rows // n_tp
+        hidden = hidden // 2
+        ids = copy_ids(n_sp, width // 512)
         V = pltpu.VMEM
         any_spec = pl.BlockSpec(memory_space=pl.ANY)
         vm = pl.BlockSpec(memory_space=pltpu.VMEM)
@@ -435,15 +460,17 @@
             out_specs=vm,
             scratch_shapes=[
                 V((width, hidden), BF16), V((width, hidden), BF16),
-                V((rows, hidden), BF16), V((rows, width), BF16),
+                V((2 * rows, hidden), BF16), V((2 * rows, width), BF16),
                 V((rows, width), BF16), V((n_tp, own, width), BF16),
-                V((rows, width), BF16), V((n_tp, own, width), BF16),
+                V((2 * rows, width), BF16), V((n_tp, 2 * own, width), BF16),
+                V((own, width), BF16), V((own, width), BF16),
                 V((ch // 128, rows, 128), F32), V((ch // 128, rows, 128), F32), V((rows + 8, ch), F32),
                 V((rows, ch), BF16), V((rows, ch), BF16), V((rows, ch), BF16),
                 V((rows, ch), F32), V((ch, width), BF16), V((own, width), BF16),
                 V((16, ch), BF16), V((n_sp, 8, ch), F32), V((SCAN, 8, ch), F32),
                 V((own, width), BF16), V((2, ch // 128, 128, 128), BF16),
                 dma((len(ids),)), dma((len(ids),)), dma((3, n_tp)), dma((3, n_tp)),
+                dma((2 * width // 512, n_tp)), dma((2 * width // 512, n_tp)),
                 dma((n_sp,)), dma((n_sp,)), dma((7,)),
             ],
             compiler_params=pltpu.CompilerParams(

time: 205 us -> 179 us (0.87)
  Pallas kernels: 203 us -> 176 us
    pallas_call x1, Pallas kernels: 203 us -> 176 us  [local(): pl.pallas_call(functools.partial(kernel, (n_sp, n_tp, ids)), out_shape=ja...]
where the time goes in v3:
time: 179 us; the launch traced here: 178 us
  Pallas kernels  176 us (98%)
  local copies, waits for them, and re-layouts  1.88 us (1%)
    pallas_call x1, Pallas kernels, local(): pl.pallas_call(functools.partial(kernel, (n_sp, n_tp, ids)), out_shape=ja...  176 us

profile of v3, /device:TPU:0, one launch (start us, length us, event | category | flops | bytes accessed | tf_op | source)
XLA Modules:
  0.0 177.9 jit_solution(11049540322671601971)
XLA Ops:
  0.0 176.0 %shard_map.118 = bf16[128,2048]{1,0:T(8,128)(2,1)} custom-call(bf16[512,2048]{1,0:T(8,128)(2,1)} %res_hbm.1, bf16[512,512]{1,0:T(8,128)(2,1)} %gate_hbm.1, bf16[512,512]{1,0:T(8,128)(2,1)} %value_hbm.1, f32[4,512]{1,0:T(4,128)} %conv_ref.1, bf16[8,64,64]{2,1,0:T(8,128)(2,1)} %rate_ref.1, bf16[8,64,64]{2,1,0:T(8,128)(2,1)} %inp_ref.1, f32[1,512]{1,0:T(1,128)} %bitcast.3, ...), custom_call_target="tpu_custom_call" | custom-call | tf_op jit(solution)/shard_map/pallas_call | solution.py:455
  176.0 1.9 %copy.14 = bf16[128,2048]{1,0:T(8,128)(2,1)} copy(bf16[128,2048]{1,0:T(8,128)(2,1)} %shard_map.118) | data formatting | bytes 1048576

commit v4 on v3

--- a/solution.py
+++ b/solution.py
@@ -25,7 +25,7 @@
     res_hbm, gate_hbm, value_hbm, conv_ref, rate_ref, inp_ref, decay_ref, step_hbm,
     outw_hbm, gain_ref, up_hbm, down_hbm,
     out_ref,
-    up_all, down_all, act, normed, part, part_in, fin, fin_in, far_out, far_in,
+    up_all, down_all, act, normed, part, part_in, fin, fin_in, pair_in, far_out, far_in,
     keep, drive, pad, gated, gate_v, value_v, step_v, outw_v, res_v, halo, tot, ent,
     upd, wpair, send, recv, tsend, trecv, fsend, frecv, csend, crecv, local_sem,
 ):
@@ -309,26 +309,43 @@
     far_mine = pl.ds(pl.multiple_of(rows + tp * own, own), own)
     launch(("n",), normed.at[mine, :], normed.at[far_mine, :], (partner, tp))
 
-    def share(span, turn):
-        copies = []
-        for d in range(1, n_tp):
-            copy = pltpu.make_async_remote_copy(
-                src_ref=normed.at[span, :], dst_ref=normed.at[span, :],
-                send_sem=tsend.at[turn, d], recv_sem=trecv.at[turn, d],
-                device_id=(me, lax.rem(tp + d, n_tp)), device_id_type=MESH,
-            )
-            copy.start()
-            copies.append(copy)
-        return copies
-
-    shares = share(mine, 1)
+    pairs = n_tp // 2
+    pair, side_of = tp // 2, lax.rem(tp, 2)
+    mate = pair * 2 + 1 - side_of
+
+    def share_to(owner, base, turn, n, target):
+        span = pl.ds(pl.multiple_of(base + owner * own, own), own)
+        copy = pltpu.make_async_remote_copy(
+            src_ref=normed.at[span, :], dst_ref=normed.at[span, :],
+            send_sem=tsend.at[turn, n], recv_sem=trecv.at[turn, n],
+            device_id=(me, target), device_id_type=MESH,
+        )
+        copy.start()
+        return copy
+
+    def share(base, turn):
+        copies = [
+            share_to(tp, base, turn, j, lax.rem(tp + 2 * j, n_tp)) for j in range(1, pairs)
+        ]
+        return [share_to(tp, base, turn, 0, mate)] + copies
+
+    def pass_on(copies, base, turn):
+        more = []
+        for j in range(1, pairs):
+            copies[j].wait_recv()
+            owner = lax.rem(tp - 2 * j + n_tp, n_tp)
+            more.append(share_to(owner, base, turn, pairs - 1 + j, mate))
+        return more
+
+    shares = share(0, 1)
     take(("pd",))
     line("e", 1)
     across("e")
     forward("c", 1)
     forward("v", 1)
+    passed = pass_on(shares, 0, 1)
     take(("n",))
-    shares_far = share(far_mine, 2)
+    shares_far = share(rows, 2)
     forward("e", 1)
     for k in range(2, high):
         for name in ("u", "v", "c", "e"):
@@ -342,11 +359,12 @@
             for sign in (1, -1):
                 take((name, "f", k, sign))
 
+    passed_far = pass_on(shares_far, rows, 2)
     settle_stream("u")
     settle_stream("v")
     tile = 512
 
-    for copy in shares:
+    for copy in shares[:1] + passed:
         copy.wait_recv()
     def raise_rows(start):
         def one(n, c):
@@ -361,7 +379,7 @@
         lax.fori_loop(0, hidden // tile, one, 0)
 
     raise_rows(0)
-    for copy in shares_far:
+    for copy in shares_far[:1] + passed_far:
         copy.wait_recv()
     raise_rows(rows)
     settle_stream("c")
@@ -376,32 +394,62 @@
             act[base : base + rows, :], down_all[cols, :], (((1,), (1,)), ((), ())),
             preferred_element_type=F32,
         ).astype(BF16)
-        for d in range(1, n_tp):
-            peer = lax.rem(tp + d, n_tp)
+        for i in range(pairs):
+            there = pl.ds(pl.multiple_of(base + (2 * i + 1 - side_of) * own, own), own)
             copy = pltpu.make_async_remote_copy(
-                src_ref=fin.at[pl.ds(pl.multiple_of(base + peer * own, own), own), cols],
-                dst_ref=fin_in.at[tp, side * own : (side + 1) * own, cols],
-                send_sem=fsend.at[side * blocks + q, d], recv_sem=frecv.at[side * blocks + q, d],
+                src_ref=fin.at[there, cols], dst_ref=pair_in.at[side, i, :, cols],
+                send_sem=fsend.at[side * blocks + q, i], recv_sem=frecv.at[side * blocks + q, i],
+                device_id=(me, mate), device_id_type=MESH,
+            )
+            copy.start()
+            lowered[side, q, i] = copy
+
+    def combine(side, q):
+        cols = slice(q * tile, (q + 1) * tile)
+        for i in range(pairs):
+            lowered[side, q, i].wait_recv()
+        for j in range(1, pairs):
+            peer = lax.rem(tp + 2 * j, n_tp)
+            start = pl.multiple_of(side * rows + peer * own, own)
+
+            def add(r, c, start=start, peer=peer):
+                here = pl.ds(pl.multiple_of(r * slab, slab), slab)
+                there = pl.ds(pl.multiple_of(start + r * slab, slab), slab)
+                fin[there, cols] = (
+                    fin[there, cols].astype(F32)
+                    + pair_in[side, peer // 2, here, cols].astype(F32)
+                ).astype(BF16)
+                return c
+
+            lax.fori_loop(0, own // slab, add, 0)
+            n = pairs - 1 + j
+            copy = pltpu.make_async_remote_copy(
+                src_ref=fin.at[pl.ds(start, own), cols],
+                dst_ref=fin_in.at[pair, side * own : (side + 1) * own, cols],
+                send_sem=fsend.at[side * blocks + q, n], recv_sem=frecv.at[side * blocks + q, n],
                 device_id=(me, peer), device_id_type=MESH,
             )
             copy.start()
-            lowered[side, q, d] = copy
+            lowered[side, q, n] = copy
 
     def gathered(side, r, cols):
         here = pl.ds(pl.multiple_of(side * own + r * slab, slab), slab)
+        near = pl.ds(pl.multiple_of(r * slab, slab), slab)
         there = pl.ds(pl.multiple_of(side * rows + tp * own + r * slab, slab), slab)
-        total = fin[there, cols].astype(F32)
-        for d in range(1, n_tp):
-            total = total + fin_in[lax.rem(tp + d, n_tp), here, cols].astype(F32)
+        total = fin[there, cols].astype(F32) + pair_in[side, pair, near, cols].astype(F32)
+        for j in range(1, pairs):
+            total = total + fin_in[lax.rem(pair + j, pairs), here, cols].astype(F32)
         return total
 
     for side in (1, 0):
         for q in range(blocks):
             lower(side, q)
+        for q in range(blocks):
+            combine(side, q)
     for q in range(blocks):
         cols = slice(q * tile, (q + 1) * tile)
-        for d in range(1, n_tp):
-            lowered[1, q, d].wait_recv()
+        for j in range(1, pairs):
+            lowered[1, q, pairs - 1 + j].wait_recv()
 
         def far_sum(r, c, cols=cols):
             here = pl.ds(pl.multiple_of(r * slab, slab), slab)
@@ -412,8 +460,8 @@
         launch(("r", q), far_out.at[:, cols], far_in.at[:, cols], (partner, tp))
     for q in range(blocks):
         cols = slice(q * tile, (q + 1) * tile)
-        for d in range(1, n_tp):
-            lowered[0, q, d].wait_recv()
+        for j in range(1, pairs):
+            lowered[0, q, pairs - 1 + j].wait_recv()
         take(("r", q))
 
         def finish(r, c, cols=cols):
@@ -425,7 +473,7 @@
         lax.fori_loop(0, own // slab, finish, 0)
     for copy, send_if, _ in started.values():
         guarded(send_if, copy.wait_send)
-    for copy in carries + sums + shares + shares_far + list(lowered.values()):
+    for copy in carries + sums + shares + shares_far + passed + passed_far + list(lowered.values()):
         copy.wait_send()
 
 
@@ -462,7 +510,8 @@
                 V((width, hidden), BF16), V((width, hidden), BF16),
                 V((2 * rows, hidden), BF16), V((2 * rows, width), BF16),
                 V((rows, width), BF16), V((n_tp, own, width), BF16),
-                V((2 * rows, width), BF16), V((n_tp, 2 * own, width), BF16),
+                V((2 * rows, width), BF16), V((n_tp // 2, 2 * own, width), BF16),
+                V((2, n_tp // 2, own, width), BF16),
                 V((own, width), BF16), V((own, width), BF16),
                 V((ch // 128, rows, 128), F32), V((ch // 128, rows, 128), F32), V((rows + 8, ch), F32),
                 V((rows, ch), BF16), V((rows, ch), BF16), V((rows, ch), BF16),

time: 179 us -> 164 us (0.916)
  Pallas kernels: 176 us -> 162 us
    pallas_call x1, Pallas kernels: 176 us -> 162 us  [local(): pl.pallas_call(functools.partial(kernel, (n_sp, n_tp, ids)), out_shape=ja...]
where the time goes in v4:
time: 164 us
  Pallas kernels  162 us (99%)
  local copies, waits for them, and re-layouts  1.88 us (1%)
    pallas_call x1, Pallas kernels, local(): pl.pallas_call(functools.partial(kernel, (n_sp, n_tp, ids)), out_shape=ja...  162 us

profile of v4, /device:TPU:0, one launch (start us, length us, event | category | flops | bytes accessed | tf_op | source)
XLA Modules:
  0.0 163.8 jit_solution(1114945657431847302)
XLA Ops:
  0.0 161.9 %shard_map.118 = bf16[128,2048]{1,0:T(8,128)(2,1)} custom-call(bf16[512,2048]{1,0:T(8,128)(2,1)} %res_hbm.1, bf16[512,512]{1,0:T(8,128)(2,1)} %gate_hbm.1, bf16[512,512]{1,0:T(8,128)(2,1)} %value_hbm.1, f32[4,512]{1,0:T(4,128)} %conv_ref.1, bf16[8,64,64]{2,1,0:T(8,128)(2,1)} %rate_ref.1, bf16[8,64,64]{2,1,0:T(8,128)(2,1)} %inp_ref.1, f32[1,512]{1,0:T(1,128)} %bitcast.3, ...), custom_call_target="tpu_custom_call" | custom-call | tf_op jit(solution)/shard_map/pallas_call | solution.py:503
  161.9 1.9 %copy.14 = bf16[128,2048]{1,0:T(8,128)(2,1)} copy(bf16[128,2048]{1,0:T(8,128)(2,1)} %shard_map.118) | data formatting | bytes 1048576
